TPU v7x, 512 devices: a whole 4x8x8 slice. The times are simulated.
512 devices in a mesh: sp: 64 (over z, y), fs: 4 (over x), tp: 2 (over core).
Axes of the slice: x: 4, y: 8, z: 8, core: 2. Of those that a mesh axis runs over, the one named last changes fastest.
Arguments:
- tokens: bfloat16 [32768, 2048], P(('fs', 'sp')), may hold values from -6 to 6
- in_gain: float32 [2048], replicated, may hold values from 0.1 to 1.9
- query_weight: bfloat16 [2048, 512], P(None, ('tp', 'fs')), may hold values from -0.17291713 to 0.17291713
- key_weight: bfloat16 [2048, 512], P(None, ('tp', 'fs')), may hold values from -0.17291713 to 0.17291713
- value_weight: bfloat16 [2048, 512], P(None, ('tp', 'fs')), may hold values from -0.125 to 0.125
- rec_query_weight: bfloat16 [2048, 512], P(None, ('tp', 'fs')), may hold values from -0.125 to 0.125
- rec_forget_weight: bfloat16 [2048, 512], P(None, ('tp', 'fs')), may hold values from -0.125 to 0.125
- rec_input_weight: bfloat16 [2048, 512], P(None, ('tp', 'fs')), may hold values from -0.125 to 0.125
- mix_lambda: float32 [4], P('tp'), may hold values from 0.3 to 0.8
- lower_bound: float32 [4, 128], P('tp'), may hold values from 0.9 to 0.9999695
- forget_scale: float32 [32768], P(('fs', 'sp')), may hold values from 0.35 to 24576
- att_gain: float32 [128], replicated, may hold values from 0.1 to 1.9
- recurrence_gain: float32 [128], replicated, may hold values from 0.1 to 1.9
- att_out_weight: bfloat16 [512, 2048], P('tp'), may hold values from -0.1875 to 0.1875
- rec_out_weight: bfloat16 [512, 2048], P('tp'), may hold values from -0.1875 to 0.1875
Outputs:
- mixed_out: bfloat16 [32768, 2048], P(('fs', 'sp'))
- log_weight_sum: float32 [4, 32768], P('tp', ('fs', 'sp'))
All inputs are finite; a program needn't handle non-finite values.
Results may differ from a plain program's by a relative error of at most 0.012.
Values may be sent and summed in bfloat16 or wider, within the bound.
A program may use at most 128 MiB of HBM per device.

v0:
```python
import jax
import jax.numpy as jnp
from jax import lax
from jax.sharding import Mesh
from jax.sharding import PartitionSpec as P

DK = 64
DV = 128
BLK = 64
SP = ("sp_0", "sp_1")
FS_SP = ("fs", "sp_0", "sp_1")
EPS = 1e-06
NEG = -1e30


def in_one_piece(arrays, axis, dim, along):
    widths = [a.shape[along] for a in arrays]
    both = jnp.concatenate(arrays, axis=along)
    filled = lax.all_gather(both, axis, axis=dim, tiled=True)
    return tuple(jnp.split(filled, [sum(widths[:k]) for k in range(1, len(widths))], axis=along))


def nothing_yet(x, identity):
    return jax.tree.map(
        lambda part, zero: jnp.zeros_like(part) + jnp.asarray(zero, part.dtype), x, identity
    )


def entering(x, axes, combine, identity):
    before = start = nothing_yet(x, identity)
    running = x
    for axis in reversed(axes):
        peers, here = (lax.axis_size(axis), lax.axis_index(axis))
        pieces = jax.tree.map(lambda part: lax.all_gather(part, axis), running)
        inside, running = (start, start)
        for k in range(peers):
            passed = k < here
            running = combine(running, jax.tree.map(lambda part: part[k], pieces))
            inside = jax.tree.map(lambda new, old: jnp.where(passed, new, old), running, inside)
        before = combine(inside, before)
    return before


def copy_for_each(x, axis):
    peers = lax.axis_size(axis)
    return lax.all_to_all(jnp.broadcast_to(x[None], (peers, *x.shape)), axis, 0, 0, tiled=True)


def taken_together(x, axis):
    return copy_for_each(x, axis).astype(jnp.float32).sum(axis=0)


def norm_rows(values, gain):
    return values * lax.rsqrt(jnp.mean(values * values, axis=-1, keepdims=True) + EPS) * gain


def block_recurrence(queries, key_in, value_in, log_forget):
    head_count, row_count, key_width = queries.shape
    block_count = row_count // BLK

    def to_blocks(array_in):
        return array_in.reshape(head_count, block_count, BLK, array_in.shape[-1]).transpose(
            1, 0, 2, 3
        )

    causal = jnp.tril(jnp.ones((BLK, BLK), bool))

    def advance(passed_state, inputs):
        query_block, key_block, value_block, l_blk = inputs
        accumulator_sum = jnp.cumsum(l_blk, axis=1)
        cross_block_output = jnp.einsum(
            "sre,sei->sri",
            query_block * jnp.exp(accumulator_sum),
            passed_state,
            precision=lax.Precision.HIGHEST,
        )
        spread = accumulator_sum[:, :, None, :] - accumulator_sum[:, None, :, :]
        decay = jnp.exp(jnp.where(causal[None, :, :, None], spread, -jnp.inf))
        scores = jnp.einsum(
            "htk,htsk,hsk->hts", query_block, decay, key_block, precision=lax.Precision.HIGHEST
        )
        result = cross_block_output + jnp.einsum(
            "hts,hsv->htv", scores, value_block, precision=lax.Precision.HIGHEST
        )
        final_log_sum = accumulator_sum[:, -1:, :]
        updated_state = jnp.exp(final_log_sum[:, 0, :])[:, :, None] * passed_state + jnp.einsum(
            "plf,plt->pft",
            key_block * jnp.exp(final_log_sum - accumulator_sum),
            value_block,
            precision=lax.Precision.HIGHEST,
        )
        return (updated_state, result)

    begin_state = jnp.zeros((head_count, key_width, value_in.shape[-1]), jnp.float32)
    end_state, results = lax.scan(
        advance,
        begin_state,
        (to_blocks(queries), to_blocks(key_in), to_blocks(value_in), to_blocks(log_forget)),
    )
    return (
        end_state,
        results.transpose(1, 0, 2, 3).reshape(head_count, row_count, value_in.shape[-1]),
    )


def attend(online, queries, pair_keys, pair_values, allowed):
    running_max, weight_sum, numer_sum = online
    local_heads = numer_sum.shape[0]
    key_rows = pair_keys.shape[0]
    key_heads = pair_keys.reshape(key_rows, local_heads, 2, DK).transpose(1, 2, 0, 3)
    head_values = pair_values.reshape(key_rows, local_heads, DV).transpose(1, 0, 2)
    scores = jnp.einsum(
        "hmqd,hmkd->hmqk", queries, key_heads, preferred_element_type=jnp.float32
    ) * DK ** (-0.5)
    scores = jnp.where(allowed, scores, NEG)
    highest = jnp.maximum(running_max, jnp.max(scores, axis=-1))
    weights = jnp.exp(scores - highest[..., None])
    weight_sum = jnp.sum(weights, axis=-1)
    numer_sum = jnp.einsum(
        "itap,ipn->itan",
        weights.astype(jnp.bfloat16),
        head_values,
        preferred_element_type=jnp.float32,
    )
    return (highest, weight_sum, numer_sum)


def on_device(
    tokens,
    in_gain,
    query_weight,
    key_weight,
    value_weight,
    rec_query_weight,
    rec_forget_weight,
    rec_input_weight,
    mix_lambda,
    lower_bound,
    forget_scale,
    att_gain,
    recurrence_gain,
    att_out_weight,
    rec_out_weight,
):
    normed = norm_rows(tokens.astype(jnp.float32), in_gain).astype(jnp.bfloat16)
    row_count = normed.shape[0]
    stacked = jnp.stack(
        [
            query_weight,
            key_weight,
            value_weight,
            rec_query_weight,
            rec_forget_weight,
            rec_input_weight,
        ],
        axis=1,
    )
    projected = jnp.einsum(
        "rd,dnc->rnc",
        normed,
        lax.all_gather(stacked, "fs", axis=2, tiled=True),
        preferred_element_type=jnp.float32,
    ).astype(jnp.bfloat16)
    local_heads = projected.shape[2] // DV
    position = lax.axis_index(SP)
    query_pos = position * row_count + jnp.arange(row_count)
    queries = projected[:, 0].reshape(row_count, local_heads, 2, DK).transpose(1, 2, 0, 3)
    online = (
        jnp.full((local_heads, 2, row_count), NEG, jnp.float32),
        jnp.zeros((local_heads, 2, row_count), jnp.float32),
        jnp.zeros((local_heads, 2, row_count, DV), jnp.float32),
    )
    pair_keys, pair_values = in_one_piece((projected[:, 1], projected[:, 2]), SP, 0, 1)
    key_pos = jnp.arange(pair_keys.shape[0])
    allowed = query_pos[:, None] >= key_pos[None, :]
    online = lax.cond(
        jnp.int32(0) <= query_pos[-1],
        lambda state: attend(state, queries, pair_keys, pair_values, allowed),
        lambda state: state,
        online,
    )
    running_max, weight_sum, numer_sum = online
    mixed_heads = (
        numer_sum[:, 0] / weight_sum[:, 0, :, None]
        - mix_lambda[:, None, None] * numer_sum[:, 1] / weight_sum[:, 1, :, None]
    )
    att_heads = (norm_rows(mixed_heads, att_gain) * 0.8).astype(jnp.bfloat16)
    att_rows = att_heads.transpose(1, 0, 2).reshape(row_count, local_heads * DV)
    log_weight_sum = running_max[:, 0] + jnp.log(weight_sum[:, 0])

    def heads_first(array_in):
        return array_in.reshape(row_count, local_heads, DV).transpose(1, 0, 2).astype(jnp.float32)

    recurrent_queries = heads_first(projected[:, 3])
    lower_edge = lower_bound[:, None, :]
    forget = lower_edge + (1.0 - lower_edge) * jax.nn.sigmoid(heads_first(projected[:, 4]))
    log_forget = forget_scale[None, :, None] * jnp.log(forget)
    key_in = 1.0 - jnp.exp(log_forget)
    end_state, local_result = block_recurrence(
        recurrent_queries, key_in, heads_first(projected[:, 5]), log_forget
    )
    running_state = jnp.cumsum(log_forget, axis=1)
    carry_rate = jnp.exp(running_state[:, -1, :])

    def combine(earlier, later):
        return (later[0] * earlier[0], later[0][..., None] * earlier[1] + later[1])

    identity = (jnp.ones_like(carry_rate), jnp.zeros_like(end_state))
    _, incoming_state = entering((carry_rate, end_state), SP, combine, identity)
    combined = local_result + jnp.einsum(
        "zed,zdp->zep",
        recurrent_queries * jnp.exp(running_state),
        incoming_state,
        precision=lax.Precision.HIGHEST,
    )
    rec_heads = norm_rows(combined, recurrence_gain).astype(jnp.bfloat16)
    rec_rows = rec_heads.transpose(1, 0, 2).reshape(row_count, local_heads * DV)
    partial_value = jnp.dot(att_rows, att_out_weight, preferred_element_type=jnp.float32) + jnp.dot(
        rec_rows, rec_out_weight, preferred_element_type=jnp.float32
    )
    mixed_out = (
        taken_together(partial_value.astype(jnp.bfloat16), "tp")
        .astype(jnp.float32)
        .astype(jnp.bfloat16)
    )
    return (mixed_out, log_weight_sum)


def solution(mesh):
    finer = Mesh(
        mesh.devices.reshape(8, 8, mesh.shape["fs"], mesh.shape["tp"]), ("sp_0", "sp_1", "fs", "tp")
    )
    placed = (
        P(FS_SP, None),
        P(),
        P(None, ("tp", "fs")),
        P(None, ("tp", "fs")),
        P(None, ("tp", "fs")),
        P(None, ("tp", "fs")),
        P(None, ("tp", "fs")),
        P(None, ("tp", "fs")),
        P("tp"),
        P("tp", None),
        P(FS_SP),
        P(),
        P(),
        P("tp", None),
        P("tp", None),
    )
    return jax.shard_map(
        on_device,
        mesh=finer,
        in_specs=placed,
        out_specs=(P(FS_SP, None), P("tp", FS_SP)),
        check_vma=False,
    )
```

profile of v0, /device:TPU:1, one launch (start us, length us, event | category | flops | bytes accessed | tf_op | source)
XLA Modules:
  0.0 367.2 jit_solution(1742700413866512903)
XLA Ops:
  7.3 1.1 bitcast_dynamic-update-slice_fusion.5
  8.3 1.0 bitcast_dynamic-update-slice_fusion.4
  9.3 1.0 bitcast_dynamic-update-slice_fusion.3
  10.3 1.0 bitcast_dynamic-update-slice_fusion.2
  11.3 1.0 bitcast_dynamic-update-slice_fusion.1
  12.2 1.0 bitcast_dynamic-update-slice_fusion
  13.2 1.1 copy-done.2
  14.7 76.1 %all-gather.7.cloned.1.call-done = bf16[2048,6,256]{0,2,1:T(8,128)(2,1)} async-done(((bf16[2048,6,64]{0,2,1:T(8,128)(2,1)}), bf16[2048,6,256]{0,2,1:T(8,128)(2,1)}) %all-gather.7.cloned.1.call-update) | async-done | bytes 6291472 | tf_op jit(solution)/shard_map/all_gather | solution.py:161
  90.8 5.0 %convolution_convert_fusion = bf16[128,6,256]{2,0,1:T(8,128)(2,1)S(1)} fusion(bf16[2048,6,256]{0,2,1:T(8,128)(2,1)} %all-gather.7.cloned.1.call-done, bf16[128,2048]{1,0:T(8,128)(2,1)S(1)} %copy-done.3, f32[2048]{0:T(1024)S(1)} %copy-done.5, f32[128]{0:T(128)S(1)} %add_rsqrt_fusion.2), kind=kOutput, calls=%fused_computation.55 | convolution fusion | flops 806551552 | bytes 7217664 | tf_op jit(solution)/shard_map/rd,dnc->rnc/dot_general | solution.py:158
  96.3 16.1 %while.13 = (s32[]{:T(128)}, f32[2,128,128]{2,1,0:T(8,128)S(1)}, f32[2,2,64,128]{3,2,0,1:T(8,128)S(1)}, f32[2,2,64,128]{3,2,0,1:T(8,128)S(1)}, f32[2,2,64,128]{3...) while((s32[]{:T(128)}, f32[2,128,128]{2,1,0:T(8,128)S(1)}, ...), condition=%wide.region_8.9_spmd.clone, body=%wide.region_6.8_spmd.clone.sunk | while | flops 79876096 | bytes 1819267 | solution.py:95
  96.5 6.9 %fusion.202 = f32[2,64,1,64]{3,2,1,0:T(1,128)S(1)} fusion(f32[2,64,128,1]{2,3,1,0:T(1,128)S(1)} %bitcast.358, f32[2,64,128]{2,1,0:T(8,128)S(1)} %get-tuple-element.238, f32[2,64,128]{2,1,0:T(8,128)S(1)} %reduce_window_sum.25, pred[64,64]{1,0:T(8,128)(4,1)S(1)} %iota_compare_fusion.2), kind=kOutput, calls=%fused_computation.14.clone.1 | convolution fusion | flops 15728640 | bytes 233472 | tf_op jit(solution)/shard_map/while/body/eval_jaxpr/htk,htsk,hsk->hts/dot_general | solution.py:79
  104.5 6.9 %fusion.202 = f32[2,64,1,64]{3,2,1,0:T(1,128)S(1)} fusion(f32[2,64,128,1]{2,3,1,0:T(1,128)S(1)} %bitcast.358, f32[2,64,128]{2,1,0:T(8,128)S(1)} %get-tuple-element.238, f32[2,64,128]{2,1,0:T(8,128)S(1)} %reduce_window_sum.25, pred[64,64]{1,0:T(8,128)(4,1)S(1)} %iota_compare_fusion.2), kind=kOutput, calls=%fused_computation.14.clone.1 | convolution fusion | flops 15728640 | bytes 233472 | tf_op jit(solution)/shard_map/while/body/eval_jaxpr/htk,htsk,hsk->hts/dot_general | solution.py:79
  112.4 0.6 copy-done.1
  113.3 12.4 %all-gather = f32[16,1,128]{2,1,0:T(1,128)S(1)} all-gather(f32[2,1,128]{2,1,0:T(1,128)S(1)} %slice_exponential_fusion), channel_id=2, replica_groups=mesh['sp_0'=8,'sp_1'=8,'fs'=4,'tp'=2] {'sp_1'}, dimensions={0}, use_global_device_ids=true | all-gather | bytes 9216 | tf_op jit(solution)/shard_map/all_gather | solution.py:34
  125.7 24.3 %all-gather.13.cloned.1.call-done = f32[16,128,128]{2,1,0:T(8,128)} async-done(((f32[2,128,128]{2,1,0:T(8,128)}), f32[16,128,128]{2,1,0:T(8,128)}) %all-gather.13.cloned.1.call-update) | async-done | bytes 1048592 | tf_op jit(solution)/shard_map/all_gather | solution.py:34
  150.0 2.3 bitcast_add_fusion
  152.4 0.7 pad_maximum_fusion
  154.4 13.5 %all_gather.27 = f32[8,2,128]{2,1,0:T(2,128)S(1)} all-gather(f32[1,2,128]{2,1,0:T(2,128)S(1)} %get-tuple-element.183), channel_id=1, replica_groups=mesh['sp_0'=8,'sp_1'=8,'fs'=4,'tp'=2] {'sp_0'}, dimensions={0}, use_global_device_ids=true | all-gather | bytes 9216 | tf_op jit(solution)/shard_map/all_gather | solution.py:34
  168.0 25.6 %all-gather.11.cloned.1.call-done = f32[8,2,128,128]{3,2,1,0:T(8,128)} async-done(((f32[1,2,128,128]{3,2,1,0:T(8,128)}), f32[8,2,128,128]{3,2,1,0:T(8,128)}) %all-gather.11.cloned.1.call-update) | async-done | bytes 1048592 | tf_op jit(solution)/shard_map/all_gather | solution.py:34
  193.5 2.6 multiply_reduce_fusion
  196.3 102.3 %all-gather.9.cloned.1.call-done = bf16[8192,512]{1,0:T(8,128)(2,1)} async-done(((bf16[128,512]{1,0:T(8,128)(2,1)}), bf16[8192,512]{1,0:T(8,128)(2,1)}) %all-gather.9.cloned.1.call-update) | async-done | bytes 8388624 | tf_op jit(solution)/shard_map/all_gather | solution.py:19
  299.0 53.7 %conditional.1 = (f32[2,2,128]{2,1,0:T(2,128)S(1)}, f32[2,2,128,128]{3,2,1,0:T(8,128)S(1)}, f32[2,128]{1,0:T(2,128)S(1)}) conditional(s32[]{:T(128)} %bitcast.8, () %tuple.22, (s32[]{:T(128)}, s32[128,1]{0,1:T(1,128)S(1)}, s32[128,8192]{1,0:T(8,128)S(1)}, bf16[8192,512]{1,0:T(8,128)(2,1)}, bf16[2,2,128,64]{2,3,1,0:T(8,128)(2,1)S(1)}) %tuple.88), branch_computations={%region_1.0_spmd, %region_2.5_spmd} | conditional | flops 1657798272 | bytes 109395480 | solution.py:176
  299.2 0.7 broadcast_compare_fusion
  299.9 11.9 %copy.86 = bf16[8192,512]{0,1:T(8,128)(2,1)} copy(bf16[8192,512]{1,0:T(8,128)(2,1)} %get-tuple-element.135) | data formatting | bytes 16777216 | tf_op jit(solution)/shard_map
  311.8 5.9 %fusion.173 = (bf16[8192,256]{0,1:T(8,128)(2,1)}, bf16[8192,256]{0,1:T(8,128)(2,1)}) fusion(bf16[8192,512]{0,1:T(8,128)(2,1)} %copy.86), kind=kLoop, calls=%fused_computation.242 | loop fusion | bytes 16777216 | tf_op jit(solution)/shard_map/split | solution.py:20
  317.8 6.3 %copy.84 = bf16[8192,2,128]{2,0,1:T(8,128)(2,1)} copy(bf16[8192,2,128]{0,2,1:T(8,128)(2,1)} %bitcast.357) | data formatting | bytes 8388608 | tf_op jit(solution)/shard_map/cond/branch_1_fun/reshape | solution.py:111
  324.1 11.2 %fusion.2 = (f32[2,2,128]{2,1,0:T(2,128)S(1)}, f32[2,2,128,8192]{3,2,1,0:T(8,128)}) fusion(pred[128,8192]{1,0:T(8,128)(4,1)S(1)} %broadcast_compare_fusion, bf16[2,2,128,64]{2,3,1,0:T(8,128)(2,1)S(1)} %get-tuple-element.54, bf16[2,2,8192,64]{2,3,1,0:T(8,128)(2,1)} %bitcast.361), kind=kOutput, calls=%fused_computation.3 | convolution fusion | flops 549453312 | bytes 22087680 | tf_op jit(solution)/shard_map/cond/branch_1_fun/hmqd,hmkd->hmqk/dot_general | solution.py:112
  335.3 9.3 %fusion.5 = f32[2,2,128,128]{3,2,1,0:T(8,128)S(1)} fusion(f32[2,2,128,8192]{3,2,1,0:T(8,128)} %get-tuple-element.165, f32[2,2,128]{2,1,0:T(2,128)S(1)} %broadcast_maximum_fusion, pred[128,8192]{1,0:T(8,128)(4,1)S(1)} %broadcast_compare_fusion, bf16[8192,2,128]{2,0,1:T(8,128)(2,1)} %copy.84), kind=kOutput, calls=%fused_computation.6 | convolution fusion | flops 1090519040 | bytes 22284288 | tf_op jit(solution)/shard_map/cond/branch_1_fun/itap,ipn->itan/dot_general | solution.py:119
  344.6 8.1 %fusion.4 = f32[2,2,128]{2,1,0:T(2,128)S(1)} fusion(f32[2,2,128,8192]{3,2,1,0:T(8,128)} %get-tuple-element.165, f32[2,2,128]{2,1,0:T(2,128)S(1)} %broadcast_maximum_fusion, pred[128,8192]{1,0:T(8,128)(4,1)S(1)} %broadcast_compare_fusion), kind=kLoop, calls=%fused_computation.5 | loop fusion | flops 16776704 | bytes 17829888 | tf_op jit(solution)/shard_map/cond/branch_1_fun/reduce_sum | solution.py:118
  352.9 0.6 log_add_fusion
  354.5 5.1 %all_to_all.5 = bf16[2,128,2048]{2,1,0:T(8,128)(2,1)S(1)} all-to-all(bf16[2,128,2048]{2,1,0:T(8,128)(2,1)S(1)} %broadcast_in_dim.46), channel_id=1, replica_groups=mesh['sp_0'=8,'sp_1'=8,'fs'=4,'tp'=2] {'tp'}, dimensions={0} | all-to-all | bytes 2097152 | tf_op jit(solution)/shard_map/all_to_all | solution.py:46
  359.6 1.1 reduce_sum.51
  (87 shorter events, 5.6 us)
Async XLA Ops:
  7.2 346.5 %copy-start = (bf16[256,2048]{1,0:T(8,128)(2,1)S(1)}, bf16[256,2048]{1,0:T(8,128)(2,1)}, u32[]{:S(2)}) copy-start(bf16[256,2048]{1,0:T(8,128)(2,1)} %param.32) | copy-start | bytes 3145732
  7.2 7.3 %copy-start.3 = (bf16[128,2048]{1,0:T(8,128)(2,1)S(1)}, bf16[128,2048]{1,0:T(8,128)(2,1)}, u32[]{:S(2)}) copy-start(bf16[128,2048]{1,0:T(8,128)(2,1)} %param.19) | copy-start | bytes 1572868
  7.2 7.5 %copy-start.6 = (f32[2,128]{1,0:T(2,128)S(1)}, f32[2,128]{1,0:T(2,128)}, u32[]{:S(2)}) copy-start(f32[2,128]{1,0:T(2,128)} %param.28) | copy-start | bytes 3076
  7.2 83.6 %copy-start.5 = (f32[2048]{0:T(1024)S(1)}, f32[2048]{0:T(1024)}, u32[]{:S(2)}) copy-start(f32[2048]{0:T(1024)} %param.20) | copy-start | bytes 24580
  7.2 83.6 %all-gather.7.cloned.1.call-start = ((), (), s32[]{:S(2)}) async-start(), calls=%async_computation.1 | async-start | bytes 7864320 | tf_op jit(solution)/shard_map/all_gather | solution.py:161
  13.2 1.1 copy-start.2
  14.4 135.6 %all-gather.13.cloned.1.call-start = ((), (), s32[]{:S(2)}) async-start(), calls=%async_computation.4 | async-start | bytes 1179648 | tf_op jit(solution)/shard_map/all_gather | solution.py:34
  14.7 81.5 %copy-start.7 = (f32[128]{0:T(128)S(1)}, f32[128]{0:T(128)}, u32[]{:S(2)}) copy-start(f32[128]{0:T(128)} %param.29) | copy-start | bytes 1540
  112.4 0.7 copy-start.1
  112.4 83.8 %copy-start.8 = (f32[128]{0:T(128)S(1)}, f32[128]{0:T(128)}, u32[]{:S(2)}) copy-start(f32[128]{0:T(128)} %param.31) | copy-start | bytes 1540
  113.0 80.5 %all-gather.11.cloned.1.call-start = ((), (), s32[]{:S(2)}) async-start(), calls=%async_computation.3 | async-start | bytes 1179648 | tf_op jit(solution)/shard_map/all_gather | solution.py:34
  152.3 146.3 %all-gather.9.cloned.1.call-start = ((), (), s32[]{:S(2)}) async-start(), calls=%async_computation.2 | async-start | bytes 8519680 | tf_op jit(solution)/shard_map/all_gather | solution.py:19
  299.0 54.5 %copy-start.9 = (f32[2]{0:T(128)S(1)}, f32[2]{0:T(128)}, u32[]{:S(2)}) copy-start(f32[2]{0:T(128)} %param.27) | copy-start | bytes 28
  299.0 54.6 %copy-start.10 = (f32[128]{0:T(128)S(1)}, f32[128]{0:T(128)}, u32[]{:S(2)}) copy-start(f32[128]{0:T(128)} %param.30) | copy-start | bytes 1540
  299.0 55.0 %copy-start.4 = (bf16[256,2048]{1,0:T(8,128)(2,1)S(1)}, bf16[256,2048]{1,0:T(8,128)(2,1)}, u32[]{:S(2)}) copy-start(bf16[256,2048]{1,0:T(8,128)(2,1)} %param.33) | copy-start | bytes 3145732
Sparse Core Ops, SparseCore 0:
  14.5 76.2 all-gather.6
  113.2 36.8 all-gather.12
  152.4 41.0 all-gather.10
  197.0 101.4 all-gather.8
where the time goes:
time: 368 us; the launch traced here: 367 us
  waiting for transfers between devices  228 us (62%)
  matrix products  44.4 us (12%)
  local copies, waits for them, and re-layouts  33.7 us (9%)
  blocking collectives  31 us (8%)
  between operations  14.8 us (4%)
  other arithmetic  14.5 us (4%)
    all_gather x1, waiting for transfers between devices, in_one_piece(): filled = lax.all_gather(both, axis, axis=dim, tiled=True)  102 us
    all_gather x1, waiting for transfers between devices, on_device(): lax.all_gather(stacked, 'fs', axis=2, tiled=True)  76.1 us
    all_gather x2, waiting for transfers between devices, entering(): pieces = jax.tree.map(lambda part: lax.all_gather(part, axis), running)  49.9 us
    all_gather x2, blocking collectives, entering(): pieces = jax.tree.map(lambda part: lax.all_gather(part, axis), running)  25.9 us
    dot_general x2, matrix products, advance(): jnp.einsum('htk,htsk,hsk->hts', query_block, decay, key_block, precision=...  13.9 us
    another operation x1, local copies, waits for them, and re-layouts  11.9 us
    dot_general x1, matrix products, attend(): jnp.einsum('hmqd,hmkd->hmqk', queries, key_heads, preferred_element_type=...  11.2 us
    dot_general x1, matrix products, attend(): jnp.einsum('itap,ipn->itan', weights.astype(jnp.bfloat16), head_values, p...  9.28 us
  transfers between devices with their start and end apart: 4, of which 4 were waited for; matrix products, arithmetic and copies ran while one was open for 1% of the time, Pallas kernels for 0%

commit v1 on v0

--- a/solution.py
+++ b/solution.py
@@ -1,3 +1,4 @@
+import functools
 import jax
 import jax.numpy as jnp
 from jax import lax
@@ -11,6 +12,19 @@
 FS_SP = ("fs", "sp_0", "sp_1")
 EPS = 1e-06
 NEG = -1e30
+
+
+def treat_the_islands(local_block, where_dim):
+    return jax.lax.all_to_all(
+        jnp.concatenate([local_block for _ in range(jax.lax.psum(1, "fs"))], axis=where_dim),
+        "fs",
+        where_dim,
+        where_dim,
+        tiled=True,
+    )
+
+
+state_edges = functools.partial(treat_the_islands, where_dim=2)
 
 
 def in_one_piece(arrays, axis, dim, along):
@@ -156,10 +170,7 @@
         axis=1,
     )
     projected = jnp.einsum(
-        "rd,dnc->rnc",
-        normed,
-        lax.all_gather(stacked, "fs", axis=2, tiled=True),
-        preferred_element_type=jnp.float32,
+        "rd,dnc->rnc", normed, state_edges(stacked), preferred_element_type=jnp.float32
     ).astype(jnp.bfloat16)
     local_heads = projected.shape[2] // DV
     position = lax.axis_index(SP)

time: 368 us -> 403 us (1.095)
  waiting for transfers between devices: 228 us -> 242 us
  blocking collectives: 31 us -> 37.7 us
  starting transfers between devices: 0.16 us -> 6.07 us
  local copies, waits for them, and re-layouts: 33.7 us -> 39.5 us
    all_to_all x0 -> x1, waiting for transfers between devices: none -> 87.8 us  [treat_the_islands(): jax.lax.all_to_all(jnp.concatenate([local_block for _ in range(jax.lax.ps...]
    all_gather x1 -> x0, waiting for transfers between devices: 76.1 us -> none  [on_device(): lax.all_gather(stacked, 'fs', axis=2, tiled=True)]
    concatenate x0 -> x1, local copies, waits for them, and re-layouts: none -> 6.87 us  [treat_the_islands(): jnp.concatenate([local_block for _ in range(jax.lax.psum(1, 'fs'))], axis...]
    all_gather x2, blocking collectives: 25.9 us -> 32.5 us  [entering(): pieces = jax.tree.map(lambda part: lax.all_gather(part, axis), running)]
    all_to_all x0 -> x1, starting transfers between devices: none -> 5.77 us  [treat_the_islands(): jax.lax.all_to_all(jnp.concatenate([local_block for _ in range(jax.lax.ps...]
where the time goes in v1:
time: 403 us; the launch traced here: 402 us
  waiting for transfers between devices  242 us (60%)
  matrix products  46.7 us (12%)
  local copies, waits for them, and re-layouts  39.5 us (10%)
  blocking collectives  37.7 us (9%)
  other arithmetic  15.2 us (4%)
  between operations  14.7 us (4%)
  starting transfers between devices  6.07 us (2%)
    all_gather x1, waiting for transfers between devices, in_one_piece(): filled = lax.all_gather(both, axis, axis=dim, tiled=True)  102 us
    all_to_all x1, waiting for transfers between devices, treat_the_islands(): jax.lax.all_to_all(jnp.concatenate([local_block for _ in range(jax.lax.ps...  87.8 us
    all_gather x2, waiting for transfers between devices, entering(): pieces = jax.tree.map(lambda part: lax.all_gather(part, axis), running)  51.8 us
    all_gather x2, blocking collectives, entering(): pieces = jax.tree.map(lambda part: lax.all_gather(part, axis), running)  32.5 us
    dot_general x2, matrix products, advance(): jnp.einsum('htk,htsk,hsk->hts', query_block, decay, key_block, precision=...  13.9 us
    another operation x1, local copies, waits for them, and re-layouts  12 us
    dot_general x1, matrix products, attend(): jnp.einsum('hmqd,hmkd->hmqk', queries, key_heads, preferred_element_type=...  11.2 us
    dot_general x1, matrix products, attend(): jnp.einsum('itap,ipn->itan', weights.astype(jnp.bfloat16), head_values, p...  9.29 us
  transfers between devices with their start and end apart: 4, of which 4 were waited for; matrix products, arithmetic and copies ran while one was open for 1% of the time, Pallas kernels for 0%

profile of v1, /device:TPU:1, one launch (start us, length us, event | category | flops | bytes accessed | tf_op | source)
XLA Modules:
  0.0 402.2 jit_solution(13919195507270002177)
XLA Ops:
  7.2 1.1 bitcast_dynamic-update-slice_fusion.5
  8.2 1.0 bitcast_dynamic-update-slice_fusion.4
  9.2 1.0 bitcast_dynamic-update-slice_fusion.3
  10.2 1.0 bitcast_dynamic-update-slice_fusion.2
  11.2 1.0 bitcast_dynamic-update-slice_fusion.1
  12.1 1.0 bitcast_dynamic-update-slice_fusion
  13.1 0.8 pad_maximum_fusion
  13.9 6.9 %copy.124 = bf16[2048,6,256]{0,1,2:T(8,128)(2,1)} copy(bf16[2048,6,256]{0,2,1:T(8,128)(2,1)S(1)} %pad_maximum_fusion) | data formatting | bytes 12582912 | tf_op jit(solution)/shard_map/concatenate | solution.py:19
  20.8 5.8 %all-to-all-start = ((bf16[2048,6,256]{0,1,2:T(8,128)(2,1)}), bf16[2048,6,256]{0,1,2:T(8,128)(2,1)}, u32[]{:S(2)}, u32[]{:S(2)}) async-start(bf16[2048,6,256]{0,1,2:T(8,128)(2,1)} %copy.124), calls=%async_computation | async-start | bytes 16777216 | tf_op jit(solution)/shard_map/all_to_all | solution.py:18
  27.0 87.8 %all-to-all-done = bf16[2048,6,256]{0,1,2:T(8,128)(2,1)} async-done(((bf16[2048,6,256]{0,1,2:T(8,128)(2,1)}), bf16[2048,6,256]{0,1,2:T(8,128)(2,1)}, u32[]{:S(2)}, u32[]{:S(2)}) %all-to-all-start) | async-done | bytes 6291488 | tf_op jit(solution)/shard_map/all_to_all | solution.py:18
  114.8 7.3 %fusion.44 = bf16[128,6,256]{2,0,1:T(8,128)(2,1)S(1)} fusion(bf16[2048,6,256]{0,1,2:T(8,128)(2,1)} %all-to-all-done, bf16[128,2048]{1,0:T(8,128)(2,1)S(1)} %copy-done.3, f32[2048]{0:T(1024)S(1)} %copy-done.9, f32[128]{0:T(128)S(1)} %add_rsqrt_fusion.2), kind=kOutput, calls=%fused_computation.58 | convolution fusion | flops 806551552 | bytes 7217664 | tf_op jit(solution)/shard_map/rd,dnc->rnc/dot_general | solution.py:172
  122.6 16.1 %while.13 = (s32[]{:T(128)}, f32[2,128,128]{2,1,0:T(8,128)S(1)}, f32[2,2,64,128]{3,2,0,1:T(8,128)S(1)}, f32[2,2,64,128]{3,2,0,1:T(8,128)S(1)}, f32[2,2,64,128]{3...) while((s32[]{:T(128)}, f32[2,128,128]{2,1,0:T(8,128)S(1)}, ...), condition=%wide.region_8.9_spmd.clone, body=%wide.region_6.8_spmd.clone.sunk | while | flops 79876096 | bytes 1819267 | solution.py:109
  122.8 6.9 %fusion.206 = f32[2,64,1,64]{3,2,1,0:T(1,128)S(1)} fusion(f32[2,64,128,1]{2,3,1,0:T(1,128)S(1)} %bitcast.357, f32[2,64,128]{2,1,0:T(8,128)S(1)} %get-tuple-element.250, f32[2,64,128]{2,1,0:T(8,128)S(1)} %reduce_window_sum.25, pred[64,64]{1,0:T(8,128)(4,1)S(1)} %iota_compare_fusion.2), kind=kOutput, calls=%fused_computation.14.clone.1 | convolution fusion | flops 15728640 | bytes 233472 | tf_op jit(solution)/shard_map/while/body/eval_jaxpr/htk,htsk,hsk->hts/dot_general | solution.py:93
  130.8 6.9 %fusion.206 = f32[2,64,1,64]{3,2,1,0:T(1,128)S(1)} fusion(f32[2,64,128,1]{2,3,1,0:T(1,128)S(1)} %bitcast.357, f32[2,64,128]{2,1,0:T(8,128)S(1)} %get-tuple-element.250, f32[2,64,128]{2,1,0:T(8,128)S(1)} %reduce_window_sum.25, pred[64,64]{1,0:T(8,128)(4,1)S(1)} %iota_compare_fusion.2), kind=kOutput, calls=%fused_computation.14.clone.1 | convolution fusion | flops 15728640 | bytes 233472 | tf_op jit(solution)/shard_map/while/body/eval_jaxpr/htk,htsk,hsk->hts/dot_general | solution.py:93
  139.6 18.8 %all-gather = f32[16,1,128]{2,1,0:T(1,128)S(1)} all-gather(f32[2,1,128]{2,1,0:T(1,128)S(1)} %slice_exponential_fusion), channel_id=2, replica_groups=mesh['sp_0'=8,'sp_1'=8,'fs'=4,'tp'=2] {'sp_1'}, dimensions={0}, use_global_device_ids=true | all-gather | bytes 9216 | tf_op jit(solution)/shard_map/all_gather | solution.py:48
  158.5 26.4 %all-gather.10.cloned.1.call-done = f32[16,128,128]{2,1,0:T(8,128)} async-done(((f32[2,128,128]{2,1,0:T(8,128)}), f32[16,128,128]{2,1,0:T(8,128)}) %all-gather.10.cloned.1.call-update) | async-done | bytes 1048592 | tf_op jit(solution)/shard_map/all_gather | solution.py:48
  184.9 2.3 bitcast_add_fusion
  187.2 0.7 pad_maximum_fusion.1
  189.3 13.7 %all_gather.23 = f32[8,2,128]{2,1,0:T(2,128)S(1)} all-gather(f32[1,2,128]{2,1,0:T(2,128)S(1)} %get-tuple-element.195), channel_id=1, replica_groups=mesh['sp_0'=8,'sp_1'=8,'fs'=4,'tp'=2] {'sp_0'}, dimensions={0}, use_global_device_ids=true | all-gather | bytes 9216 | tf_op jit(solution)/shard_map/all_gather | solution.py:48
  203.1 25.4 %all-gather.8.cloned.1.call-done = f32[8,2,128,128]{3,2,1,0:T(8,128)} async-done(((f32[1,2,128,128]{3,2,1,0:T(8,128)}), f32[8,2,128,128]{3,2,1,0:T(8,128)}) %all-gather.8.cloned.1.call-update) | async-done | bytes 1048592 | tf_op jit(solution)/shard_map/all_gather | solution.py:48
  228.4 2.6 multiply_reduce_fusion
  231.2 102.4 %all-gather.6.cloned.1.call-done = bf16[8192,512]{1,0:T(8,128)(2,1)} async-done(((bf16[128,512]{1,0:T(8,128)(2,1)}), bf16[8192,512]{1,0:T(8,128)(2,1)}) %all-gather.6.cloned.1.call-update) | async-done | bytes 8388624 | tf_op jit(solution)/shard_map/all_gather | solution.py:33
  334.1 53.6 %conditional.1 = (f32[2,2,128]{2,1,0:T(2,128)S(1)}, f32[2,2,128,128]{3,2,1,0:T(8,128)S(1)}, f32[2,128]{1,0:T(2,128)S(1)}) conditional(s32[]{:T(128)} %bitcast.8, () %tuple.22, (s32[]{:T(128)}, s32[128,1]{0,1:T(1,128)S(1)}, s32[128,8192]{1,0:T(8,128)S(1)}, bf16[8192,512]{1,0:T(8,128)(2,1)}, bf16[2,2,128,64]{2,3,1,0:T(8,128)(2,1)S(1)}) %tuple.88), branch_computations={%region_1.0_spmd, %region_2.5_spmd} | conditional | flops 1657798272 | bytes 109395480 | solution.py:187
  334.1 0.7 broadcast_compare_fusion
  334.8 12.0 %copy.127 = bf16[8192,512]{0,1:T(8,128)(2,1)} copy(bf16[8192,512]{1,0:T(8,128)(2,1)} %get-tuple-element.147) | data formatting | bytes 16777216 | tf_op jit(solution)/shard_map
  346.8 6.0 %fusion.178 = (bf16[8192,256]{0,1:T(8,128)(2,1)}, bf16[8192,256]{0,1:T(8,128)(2,1)}) fusion(bf16[8192,512]{0,1:T(8,128)(2,1)} %copy.127), kind=kLoop, calls=%fused_computation.245 | loop fusion | bytes 16777216 | tf_op jit(solution)/shard_map/split | solution.py:34
  352.7 6.3 %copy.123 = bf16[8192,2,128]{2,0,1:T(8,128)(2,1)} copy(bf16[8192,2,128]{0,2,1:T(8,128)(2,1)} %bitcast.356) | data formatting | bytes 8388608 | tf_op jit(solution)/shard_map/cond/branch_1_fun/reshape | solution.py:125
  359.1 11.2 %fusion.2 = (f32[2,2,128]{2,1,0:T(2,128)S(1)}, f32[2,2,128,8192]{3,2,1,0:T(8,128)}) fusion(pred[128,8192]{1,0:T(8,128)(4,1)S(1)} %broadcast_compare_fusion, bf16[2,2,128,64]{2,3,1,0:T(8,128)(2,1)S(1)} %get-tuple-element.54, bf16[2,2,8192,64]{2,3,1,0:T(8,128)(2,1)} %bitcast.360), kind=kOutput, calls=%fused_computation.3 | convolution fusion | flops 549453312 | bytes 22087680 | tf_op jit(solution)/shard_map/cond/branch_1_fun/hmqd,hmkd->hmqk/dot_general | solution.py:126
  370.3 9.3 %fusion.5 = f32[2,2,128,128]{3,2,1,0:T(8,128)S(1)} fusion(f32[2,2,128,8192]{3,2,1,0:T(8,128)} %get-tuple-element.177, f32[2,2,128]{2,1,0:T(2,128)S(1)} %broadcast_maximum_fusion, pred[128,8192]{1,0:T(8,128)(4,1)S(1)} %broadcast_compare_fusion, bf16[8192,2,128]{2,0,1:T(8,128)(2,1)} %copy.123), kind=kOutput, calls=%fused_computation.6 | convolution fusion | flops 1090519040 | bytes 22284288 | tf_op jit(solution)/shard_map/cond/branch_1_fun/itap,ipn->itan/dot_general | solution.py:133
  379.6 8.1 %fusion.4 = f32[2,2,128]{2,1,0:T(2,128)S(1)} fusion(f32[2,2,128,8192]{3,2,1,0:T(8,128)} %get-tuple-element.177, f32[2,2,128]{2,1,0:T(2,128)S(1)} %broadcast_maximum_fusion, pred[128,8192]{1,0:T(8,128)(4,1)S(1)} %broadcast_compare_fusion), kind=kLoop, calls=%fused_computation.5 | loop fusion | flops 16776704 | bytes 17829888 | tf_op jit(solution)/shard_map/cond/branch_1_fun/reduce_sum | solution.py:132
  389.4 5.1 %all_to_all.10 = bf16[2,128,2048]{2,1,0:T(8,128)(2,1)S(1)} all-to-all(bf16[2,128,2048]{2,1,0:T(8,128)(2,1)S(1)} %broadcast_in_dim.46), channel_id=1, replica_groups=mesh['sp_0'=8,'sp_1'=8,'fs'=4,'tp'=2] {'tp'}, dimensions={0} | all-to-all | bytes 2097152 | tf_op jit(solution)/shard_map/all_to_all | solution.py:60
  394.6 1.1 reduce_sum.51
  (86 shorter events, 6.9 us)
Async XLA Ops:
  7.2 381.5 %copy-start = (bf16[256,2048]{1,0:T(8,128)(2,1)S(1)}, bf16[256,2048]{1,0:T(8,128)(2,1)}, u32[]{:S(2)}) copy-start(bf16[256,2048]{1,0:T(8,128)(2,1)} %param.32) | copy-start | bytes 3145732
  20.7 6.0 %copy-start.3 = (bf16[128,2048]{1,0:T(8,128)(2,1)S(1)}, bf16[128,2048]{1,0:T(8,128)(2,1)}, u32[]{:S(2)}) copy-start(bf16[128,2048]{1,0:T(8,128)(2,1)} %param.19) | copy-start | bytes 1572868
  20.7 6.2 %copy-start.4 = (f32[2,128]{1,0:T(2,128)S(1)}, f32[2,128]{1,0:T(2,128)}, u32[]{:S(2)}) copy-start(f32[2,128]{1,0:T(2,128)} %param.28) | copy-start | bytes 3076
  20.8 94.0 %copy-start.9 = (f32[2048]{0:T(1024)S(1)}, f32[2048]{0:T(1024)}, u32[]{:S(2)}) copy-start(f32[2048]{0:T(1024)} %param.20) | copy-start | bytes 24580
  20.8 94.0 %all-to-all-start = ((bf16[2048,6,256]{0,1,2:T(8,128)(2,1)}), bf16[2048,6,256]{0,1,2:T(8,128)(2,1)}, u32[]{:S(2)}, u32[]{:S(2)}) async-start(bf16[2048,6,256]{0,1,2:T(8,128)(2,1)} %copy.124), calls=%async_computation | async-start | bytes 16777216 | tf_op jit(solution)/shard_map/all_to_all | solution.py:18
  26.5 158.4 %all-gather.10.cloned.1.call-start = ((), (), s32[]{:S(2)}) async-start(), calls=%async_computation.4 | async-start | bytes 1179648 | tf_op jit(solution)/shard_map/all_gather | solution.py:48
  27.0 95.5 %copy-start.5 = (f32[128]{0:T(128)S(1)}, f32[128]{0:T(128)}, u32[]{:S(2)}) copy-start(f32[128]{0:T(128)} %param.29) | copy-start | bytes 1540
  122.6 108.5 %copy-start.6 = (f32[128]{0:T(128)S(1)}, f32[128]{0:T(128)}, u32[]{:S(2)}) copy-start(f32[128]{0:T(128)} %param.31) | copy-start | bytes 1540
  138.7 0.7 copy-start.1
  139.4 89.1 %all-gather.8.cloned.1.call-start = ((), (), s32[]{:S(2)}) async-start(), calls=%async_computation.3 | async-start | bytes 1179648 | tf_op jit(solution)/shard_map/all_gather | solution.py:48
  187.2 146.4 %all-gather.6.cloned.1.call-start = ((), (), s32[]{:S(2)}) async-start(), calls=%async_computation.2 | async-start | bytes 8519680 | tf_op jit(solution)/shard_map/all_gather | solution.py:33
  334.0 54.4 %copy-start.7 = (f32[2]{0:T(128)S(1)}, f32[2]{0:T(128)}, u32[]{:S(2)}) copy-start(f32[2]{0:T(128)} %param.27) | copy-start | bytes 28
  334.1 54.5 %copy-start.8 = (f32[128]{0:T(128)S(1)}, f32[128]{0:T(128)}, u32[]{:S(2)}) copy-start(f32[128]{0:T(128)} %param.30) | copy-start | bytes 1540
  334.1 54.9 %copy-start.2 = (bf16[256,2048]{1,0:T(8,128)(2,1)S(1)}, bf16[256,2048]{1,0:T(8,128)(2,1)}, u32[]{:S(2)}) copy-start(bf16[256,2048]{1,0:T(8,128)(2,1)} %param.33) | copy-start | bytes 3145732
Sparse Core Ops, SparseCore 0:
  139.5 45.3 all-gather.9
  187.3 41.0 all-gather.7
  232.1 101.5 all-gather.5
